TPU v7x, 32 devices: a whole 2x2x4 slice. The times are simulated.
32 devices in a mesh: sp: 8 (over z, y), tp: 4 (over x, core).
Axes of the slice: x: 2, y: 2, z: 4, core: 2. Of those that a mesh axis runs over, the one named last changes fastest.
Arguments:
- source: bfloat16 [4096, 2048], P(('sp', 'tp')), may hold values from -6 to 6
- target: bfloat16 [1024, 2048], P(('sp', 'tp')), may hold values from -6 to 6
- source_gain: bfloat16 [2, 2048], replicated, may hold values from 0.099609375 to 1.8984375
- target_gain: bfloat16 [2, 2048], replicated, may hold values from 0.099609375 to 1.8984375
- query_weight: bfloat16 [2, 2048, 1024], P(None, None, 'tp'), may hold values from -0.5 to 0.5
- key_weight: bfloat16 [2, 2048, 1024], P(None, None, 'tp'), may hold values from -0.5 to 0.5
- value_weight: bfloat16 [2, 2048, 1024], P(None, None, 'tp'), may hold values from -0.125 to 0.125
- head_gain: bfloat16 [2, 1024], P(None, 'tp'), may hold values from 0.099609375 to 1.8984375
- out_weight: bfloat16 [2, 1024, 2048], P(None, 'tp'), may hold values from -0.1875 to 0.1875
- mlp_gain: bfloat16 [2048], replicated, may hold values from 0.099609375 to 1.8984375
- gate_weight: bfloat16 [2048, 5632], P(None, 'tp'), may hold values from -0.125 to 0.125
- up_weight: bfloat16 [2048, 5632], P(None, 'tp'), may hold values from -0.125 to 0.125
- down_weight: bfloat16 [5632, 2048], P('tp'), may hold values from -0.078125 to 0.078125
Outputs:
- mixed: bfloat16 [1024, 2048], P(('sp', 'tp'))
All inputs are finite; a program needn't handle non-finite values.
Results may differ from a plain program's by a relative error of at most 0.014.
Values may be sent and summed in bfloat16 or wider, within the bound.
A program may use at most 128 MiB of HBM per device.

v0:
```python
import jax
import jax.numpy as jnp
from jax import lax
from jax.sharding import PartitionSpec as P

HEAD_DIM = 128


EPSILON = 1e-06


def row_scale(rows):
    return lax.rsqrt(jnp.mean(rows * rows, axis=-1, keepdims=True) + EPSILON)


def block_stats(queries, key_blocks, value_blocks):
    scores = jnp.einsum(
        "the,bshe->bhts", queries, key_blocks, preferred_element_type=jnp.float32
    ) * HEAD_DIM ** (-0.5)
    block_max = jnp.max(scores, axis=-1)
    weights = jnp.exp(scores - block_max[..., None])
    block_total = jnp.sum(weights, axis=-1)
    block_out = jnp.einsum(
        "bhts,bshe->bthe",
        weights.astype(jnp.bfloat16),
        value_blocks,
        preferred_element_type=jnp.float32,
    ).astype(jnp.bfloat16)
    return (jnp.swapaxes(block_max, 1, 2), jnp.swapaxes(block_total, 1, 2), block_out)


def merge_blocks(carry, stats):
    run_max, run_total, run_out = carry
    block_max, block_total, block_out = stats
    new_max = jnp.max(block_max, axis=0)
    keep = jnp.exp(run_max - new_max)
    factor = jnp.exp(block_max - new_max[None])
    total = run_total * keep + jnp.sum(factor * block_total, axis=0)
    widened = lax.optimization_barrier(block_out).astype(jnp.float32)
    out = run_out * keep[..., None] + jnp.sum(factor[..., None] * widened, axis=0)
    return (new_max, total, out)


def empty_carry(row_count, head_count):
    return (
        jnp.full((row_count, head_count), -jnp.inf, jnp.float32),
        jnp.zeros((row_count, head_count), jnp.float32),
        jnp.zeros((row_count, head_count, HEAD_DIM), jnp.float32),
    )


def local(
    source,
    target,
    source_gain,
    target_gain,
    query_weight,
    key_weight,
    value_weight,
    head_gain,
    out_weight,
    mlp_gain,
    gate_weight,
    up_weight,
    down_weight,
):
    layer_count = query_weight.shape[0]
    width_local = query_weight.shape[2]
    head_count = width_local // HEAD_DIM
    own_rows = target.shape[0]
    group_rows = own_rows * lax.axis_size("tp")
    wide = lax.all_gather(source, "tp", axis=0, tiled=True).astype(jnp.float32)
    scaled = wide * row_scale(wide)
    columns = []
    for project_layer in range(layer_count):
        normed = (scaled * source_gain[project_layer].astype(jnp.float32)).astype(jnp.bfloat16)
        columns.append(
            jnp.dot(normed, key_weight[project_layer], preferred_element_type=jnp.float32).astype(
                jnp.bfloat16
            )
        )
        columns.append(
            jnp.dot(normed, value_weight[project_layer], preferred_element_type=jnp.float32).astype(
                jnp.bfloat16
            )
        )
    projected = jnp.concatenate(columns, axis=1)
    src_rows = projected.shape[0]
    state = target
    for layer in range(layer_count):
        state_wide = state.astype(jnp.float32)
        tgt_normed = (
            state_wide * row_scale(state_wide) * target_gain[layer].astype(jnp.float32)
        ).astype(jnp.bfloat16)

        def project_query(piece, start, layer=layer):
            return jnp.dot(piece, query_weight[layer], preferred_element_type=jnp.float32).astype(
                jnp.bfloat16
            )

        queries = project_query(lax.all_gather(tgt_normed, "tp", axis=0, tiled=True), jnp.int32(0))
        queries = queries.reshape(group_rows, head_count, HEAD_DIM)
        offset = 2 * layer * width_local
        keys = projected[:, offset : offset + width_local].reshape(src_rows, head_count, HEAD_DIM)
        values = projected[:, offset + width_local : offset + 2 * width_local].reshape(
            src_rows, head_count, HEAD_DIM
        )
        everyone = lax.all_gather(queries, "sp", axis=0, tiled=True)
        block_max, block_total, block_out = block_stats(everyone, keys[None], values[None])
        sp_count = lax.axis_size("sp")
        outgoing = (
            block_out.reshape(sp_count, group_rows, head_count, HEAD_DIM),
            block_max.reshape(sp_count, group_rows, head_count),
            block_total.reshape(sp_count, group_rows, head_count),
        )
        got_out = lax.all_to_all(
            outgoing[0].astype(jnp.float32), "sp", split_axis=0, concat_axis=0, tiled=True
        ).astype(jnp.bfloat16)
        got_max = lax.all_to_all(outgoing[1], "sp", split_axis=0, concat_axis=0, tiled=True)
        got_total = lax.all_to_all(outgoing[2], "sp", split_axis=0, concat_axis=0, tiled=True)
        merged = merge_blocks(
            empty_carry(got_max.shape[1], head_count), (got_max, got_total, got_out)
        )
        attended = merged[2] / merged[1][..., None]
        head_out = (
            attended
            * row_scale(attended)
            * head_gain[layer].astype(jnp.float32).reshape(head_count, HEAD_DIM)
        )
        head_out = head_out.astype(jnp.bfloat16).reshape(group_rows, width_local)

        def mix_heads(start, count, layer=layer, head_out=head_out):
            return jnp.dot(head_out, out_weight[layer], preferred_element_type=jnp.float32)

        mixed_sum = lax.psum_scatter(
            mix_heads(jnp.int32(0), own_rows * lax.axis_size("tp")),
            "tp",
            scatter_dimension=0,
            tiled=True,
        )
        state = (state.astype(jnp.float32) + mixed_sum).astype(jnp.bfloat16)
    state_wide = state.astype(jnp.float32)
    mlp_in = (state_wide * row_scale(state_wide) * mlp_gain.astype(jnp.float32)).astype(
        jnp.bfloat16
    )
    piece = lax.all_gather(mlp_in, "tp", axis=0, tiled=True)
    gate = jnp.dot(piece, gate_weight, preferred_element_type=jnp.float32)
    upward = jnp.dot(piece, up_weight, preferred_element_type=jnp.float32)
    hidden = (jax.nn.silu(gate) * upward).astype(jnp.bfloat16)
    down = lax.psum_scatter(
        jnp.dot(hidden, down_weight, preferred_element_type=jnp.float32),
        "tp",
        scatter_dimension=0,
        tiled=True,
    )
    return (state_wide + 0.5 * down).astype(jnp.bfloat16)


def solution(mesh):
    in_specs = (
        P(("sp", "tp"), None),
        P(("sp", "tp"), None),
        P(),
        P(),
        P(None, None, "tp"),
        P(None, None, "tp"),
        P(None, None, "tp"),
        P(None, "tp"),
        P(None, "tp", None),
        P(),
        P(None, "tp"),
        P(None, "tp"),
        P("tp", None),
    )
    out_specs = P(("sp", "tp"), None)
    return jax.shard_map(local, mesh=mesh, in_specs=in_specs, out_specs=out_specs, check_vma=False)
```

profile of v0, /device:TPU:0, one launch (start us, length us, event | category | flops | bytes accessed | tf_op | source)
XLA Modules:
  0.0 285.0 jit_solution(10589922507218628435)
XLA Ops:
  7.3 1.0 fusion.66
  8.3 0.8 slice_convert_fusion
  9.1 1.0 fusion.68
  10.1 8.6 %all_gather.19 = bf16[128,2048]{1,0:T(8,128)(2,1)S(1)} all-gather(bf16[32,2048]{1,0:T(8,128)(2,1)S(1)} %fusion.68), channel_id=1, replica_groups=mesh['sp'=8,'tp'=4] {'tp'}, dimensions={0}, use_global_device_ids=true | all-gather | bytes 655360 | tf_op jit(solution)/shard_map/all_gather | solution.py:101
  18.8 1.7 fusion.40
  20.5 31.6 %all_gather.20 = bf16[1024,2,128]{2,0,1:T(8,128)(2,1)S(1)} all-gather(bf16[128,2,128]{2,0,1:T(8,128)(2,1)S(1)} %bitcast.175), channel_id=1, replica_groups=mesh['sp'=8,'tp'=4] {'sp'}, dimensions={0}, use_global_device_ids=true | all-gather | bytes 589824 | tf_op jit(solution)/shard_map/all_gather | solution.py:108
  52.1 0.8 slice_convert_fusion.3
  52.9 2.1 fusion.4
  55.0 2.8 convolution_convert_fusion.3
  57.8 1.4 bitcast_reduce_fusion.1
  59.2 1.9 copy-done.1
  61.1 2.0 fusion.7
  63.1 5.6 %all-to-all-start.2 = ((f32[8,128,2]{1,2,0:T(2,128)}), f32[8,128,2]{1,2,0:T(2,128)S(1)}, u32[]{:S(2)}, u32[]{:S(2)}) async-start(f32[8,128,2]{1,2,0:T(2,128)} %bitcast.18), calls=%async_computation.2 | async-start | bytes 16384 | tf_op jit(solution)/shard_map/all_to_all | solution.py:120
  68.7 2.1 convolution_convert_fusion.2
  70.9 4.3 %all-to-all-done.2 = f32[8,128,2]{1,2,0:T(2,128)S(1)} async-done(((f32[8,128,2]{1,2,0:T(2,128)}), f32[8,128,2]{1,2,0:T(2,128)S(1)}, u32[]{:S(2)}, u32[]{:S(2)}) %all-to-all-start.2) | async-done | bytes 8224 | tf_op jit(solution)/shard_map/all_to_all | solution.py:120
  75.3 3.3 %all-to-all-start = ((f32[8,128,2]{1,2,0:T(2,128)}), f32[8,128,2]{1,2,0:T(2,128)S(1)}, u32[]{:S(2)}, u32[]{:S(2)}) async-start(f32[8,128,2]{1,2,0:T(2,128)} %bitcast.9), calls=%async_computation | async-start | bytes 16384 | tf_op jit(solution)/shard_map/all_to_all | solution.py:119
  78.6 3.1 %fusion.37 = bf16[1,2,128,1024]{3,2,1,0:T(8,128)(2,1)S(1)} fusion(bf16[512,2,128]{0,2,1:T(8,128)(2,1)S(1)} %bitcast.171, f32[2,512,1024]{2,1,0:T(8,128)} %copy-done.1, f32[2,1024]{1,0:T(2,128)} %get-tuple-element.23), kind=kOutput, calls=%fused_computation.32 | convolution fusion | flops 271843328 | bytes 4988928 | tf_op jit(solution)/shard_map/bhts,bshe->bthe/dot_general | solution.py:23
  81.8 0.9 copy.27
  82.7 2.4 all-to-all-done
  85.1 3.5 %all-to-all-start.1 = ((bf16[8,128,2,128]{1,3,2,0:T(8,128)(2,1)}), bf16[8,128,2,128]{1,3,2,0:T(8,128)(2,1)S(1)}, u32[]{:S(2)}, u32[]{:S(2)}) async-start(bf16[8,128,2,128]{1,3,2,0:T(8,128)(2,1)} %copy.27), calls=%async_computation.1 | async-start | bytes 1048576 | tf_op jit(solution)/shard_map/all_to_all | solution.py:116
  88.8 10.2 %all-to-all-done.1 = bf16[8,128,2,128]{1,3,2,0:T(8,128)(2,1)S(1)} async-done(((bf16[8,128,2,128]{1,3,2,0:T(8,128)(2,1)}), bf16[8,128,2,128]{1,3,2,0:T(8,128)(2,1)S(1)}, u32[]{:S(2)}, u32[]{:S(2)}) %all-to-all-start.1) | async-done | bytes 524320 | tf_op jit(solution)/shard_map/all_to_all | solution.py:116
  99.2 2.6 fusion.47
  101.8 2.1 convolution_convert_fusion.1
  104.0 21.4 %reduce-scatter.4.cloned.1.call-done = f32[32,2048]{1,0:T(8,128)} async-done(((f32[128,2048]{1,0:T(8,128)}), f32[32,2048]{1,0:T(8,128)}) %reduce-scatter.4.cloned.1.call-update) | async-done | bytes 262160 | tf_op jit(solution)/shard_map/reduce_scatter | solution.py:135
  125.4 1.1 fusion.70
  126.6 6.6 %all_gather.21 = bf16[128,2048]{1,0:T(8,128)(2,1)S(1)} all-gather(bf16[32,2048]{1,0:T(8,128)(2,1)S(1)} %fusion.72), channel_id=1, replica_groups=mesh['sp'=8,'tp'=4] {'tp'}, dimensions={0}, use_global_device_ids=true | all-gather | bytes 655360 | tf_op jit(solution)/shard_map/all_gather | solution.py:101
  133.2 1.5 fusion.41
  134.8 31.6 %all_gather.22 = bf16[1024,2,128]{2,0,1:T(8,128)(2,1)S(1)} all-gather(bf16[128,2,128]{2,0,1:T(8,128)(2,1)S(1)} %bitcast.176), channel_id=1, replica_groups=mesh['sp'=8,'tp'=4] {'sp'}, dimensions={0}, use_global_device_ids=true | all-gather | bytes 589824 | tf_op jit(solution)/shard_map/all_gather | solution.py:108
  166.3 1.4 bitcast_reduce_fusion
  167.7 1.9 copy-done
  169.6 2.0 fusion.9
  171.6 5.4 %all-to-all-start.5 = ((f32[8,128,2]{1,2,0:T(2,128)}), f32[8,128,2]{1,2,0:T(2,128)S(1)}, u32[]{:S(2)}, u32[]{:S(2)}) async-start(f32[8,128,2]{1,2,0:T(2,128)} %bitcast.40), calls=%async_computation.6 | async-start | bytes 16384 | tf_op jit(solution)/shard_map/all_to_all | solution.py:120
  177.0 2.1 convolution_convert_fusion
  179.1 4.4 %all-to-all-done.5 = f32[8,128,2]{1,2,0:T(2,128)S(1)} async-done(((f32[8,128,2]{1,2,0:T(2,128)}), f32[8,128,2]{1,2,0:T(2,128)S(1)}, u32[]{:S(2)}, u32[]{:S(2)}) %all-to-all-start.5) | async-done | bytes 8224 | tf_op jit(solution)/shard_map/all_to_all | solution.py:120
  183.5 3.5 %all-to-all-start.3 = ((f32[8,128,2]{1,2,0:T(2,128)}), f32[8,128,2]{1,2,0:T(2,128)S(1)}, u32[]{:S(2)}, u32[]{:S(2)}) async-start(f32[8,128,2]{1,2,0:T(2,128)} %bitcast.31), calls=%async_computation.4 | async-start | bytes 16384 | tf_op jit(solution)/shard_map/all_to_all | solution.py:119
  187.0 3.3 %fusion.31 = bf16[1,2,128,1024]{3,2,1,0:T(8,128)(2,1)S(1)} fusion(bf16[512,2,128]{0,2,1:T(8,128)(2,1)S(1)} %bitcast.170, f32[2,512,1024]{2,1,0:T(8,128)} %copy-done, f32[2,1024]{1,0:T(2,128)} %get-tuple-element.25), kind=kOutput, calls=%fused_computation.30 | convolution fusion | flops 271843328 | bytes 4988928 | tf_op jit(solution)/shard_map/bhts,bshe->bthe/dot_general | solution.py:23
  190.4 0.9 copy.32
  191.3 2.1 all-to-all-done.3
  193.4 3.7 %all-to-all-start.4 = ((bf16[8,128,2,128]{1,3,2,0:T(8,128)(2,1)}), bf16[8,128,2,128]{1,3,2,0:T(8,128)(2,1)S(1)}, u32[]{:S(2)}, u32[]{:S(2)}) async-start(bf16[8,128,2,128]{1,3,2,0:T(8,128)(2,1)} %copy.32), calls=%async_computation.5 | async-start | bytes 1048576 | tf_op jit(solution)/shard_map/all_to_all | solution.py:116
  197.2 10.2 %all-to-all-done.4 = bf16[8,128,2,128]{1,3,2,0:T(8,128)(2,1)S(1)} async-done(((bf16[8,128,2,128]{1,3,2,0:T(8,128)(2,1)}), bf16[8,128,2,128]{1,3,2,0:T(8,128)(2,1)S(1)}, u32[]{:S(2)}, u32[]{:S(2)}) %all-to-all-start.4) | async-done | bytes 524320 | tf_op jit(solution)/shard_map/all_to_all | solution.py:116
  207.6 1.3 fusion.42
  209.1 23.6 %reduce-scatter.6.cloned.1.call-done = f32[32,2048]{1,0:T(8,128)} async-done(((f32[128,2048]{1,0:T(8,128)}), f32[32,2048]{1,0:T(8,128)}) %reduce-scatter.6.cloned.1.call-update) | async-done | bytes 262160 | tf_op jit(solution)/shard_map/reduce_scatter | solution.py:135
  232.7 1.1 fusion.74
  233.9 6.6 %all_gather.23 = bf16[128,2048]{1,0:T(8,128)(2,1)S(1)} all-gather(bf16[32,2048]{1,0:T(8,128)(2,1)S(1)} %fusion.76), channel_id=1, replica_groups=mesh['sp'=8,'tp'=4] {'tp'}, dimensions={0}, use_global_device_ids=true | all-gather | bytes 655360 | tf_op jit(solution)/shard_map/all_gather | solution.py:146
  240.5 3.6 %fusion.85 = f32[128,1408]{1,0:T(8,128)S(1)} fusion(bf16[128,2048]{1,0:T(8,128)(2,1)S(1)} %all_gather.23, bf16[2048,1408]{1,0:T(8,128)(2,1)} %param.23), kind=kOutput, calls=%fused_computation.115 | convolution fusion | flops 738197504 | bytes 7012352 | tf_op jit(solution)/shard_map/dot_general | solution.py:147
  244.1 7.3 %fusion.60 = f32[128,2048]{1,0:T(8,128)} fusion(bf16[1408,2048]{1,0:T(8,128)(2,1)} %param.25, bf16[128,2048]{1,0:T(8,128)(2,1)S(1)} %all_gather.23, bf16[2048,1408]{1,0:T(8,128)(2,1)} %param.24, f32[128,1408]{1,0:T(8,128)S(1)} %fusion.85), kind=kOutput, calls=%fused_computation.61 | convolution fusion | flops 1477476352 | bytes 13828096 | tf_op jit(solution)/shard_map/dot_general | solution.py:151
  251.4 25.4 %reduce-scatter.8.cloned.1.call-done = f32[32,2048]{1,0:T(8,128)} async-done(((f32[128,2048]{1,0:T(8,128)}), f32[32,2048]{1,0:T(8,128)}) %reduce-scatter.8.cloned.1.call-update) | async-done | bytes 262160 | tf_op jit(solution)/shard_map/reduce_scatter | solution.py:150
  276.9 1.6 fusion.77
  (47 shorter events, 2.0 us)
Async XLA Ops:
  6.5 46.4 %all-gather.2.cloned.1.call-start = ((), (), s32[]{:S(2)}) async-start(), calls=%async_computation.9 | async-start | bytes 2621440 | tf_op jit(solution)/shard_map/all_gather | solution.py:72
  57.8 10.9 %copy-start.2 = (bf16[512,2048]{1,0:T(8,128)(2,1)S(1)}, bf16[512,2048]{1,0:T(8,128)(2,1)}, u32[]{:S(2)}) copy-start(bf16[512,2048]{1,0:T(8,128)(2,1)} %all-gather.2.cloned.1.call-done) | copy-start | bytes 6291460
  59.2 1.9 copy-start.1
  63.1 12.1 %all-to-all-start.2 = ((f32[8,128,2]{1,2,0:T(2,128)}), f32[8,128,2]{1,2,0:T(2,128)S(1)}, u32[]{:S(2)}, u32[]{:S(2)}) async-start(f32[8,128,2]{1,2,0:T(2,128)} %bitcast.18), calls=%async_computation.2 | async-start | bytes 16384 | tf_op jit(solution)/shard_map/all_to_all | solution.py:120
  70.9 17.8 %copy-start.6 = (bf16[2,256]{1,0:T(2,128)(2,1)S(1)}, bf16[2,256]{1,0:T(2,128)(2,1)}, u32[]{:S(2)}) copy-start(bf16[2,256]{1,0:T(2,128)(2,1)} %param.20) | copy-start | bytes 3076
  75.3 9.9 %all-to-all-start = ((f32[8,128,2]{1,2,0:T(2,128)}), f32[8,128,2]{1,2,0:T(2,128)S(1)}, u32[]{:S(2)}, u32[]{:S(2)}) async-start(f32[8,128,2]{1,2,0:T(2,128)} %bitcast.9), calls=%async_computation | async-start | bytes 16384 | tf_op jit(solution)/shard_map/all_to_all | solution.py:119
  85.1 13.8 %all-to-all-start.1 = ((bf16[8,128,2,128]{1,3,2,0:T(8,128)(2,1)}), bf16[8,128,2,128]{1,3,2,0:T(8,128)(2,1)S(1)}, u32[]{:S(2)}, u32[]{:S(2)}) async-start(bf16[8,128,2,128]{1,3,2,0:T(8,128)(2,1)} %copy.27), calls=%async_computation.1 | async-start | bytes 1048576 | tf_op jit(solution)/shard_map/all_to_all | solution.py:116
  88.7 36.7 %reduce-scatter.4.cloned.1.call-start = ((), (), s32[]{:S(2)}) async-start(), calls=%async_computation.10 | async-start | bytes 1310720 | tf_op jit(solution)/shard_map/reduce_scatter | solution.py:135
  99.2 26.1 %copy-start.4 = (bf16[32,2048]{1,0:T(8,128)(2,1)S(1)}, bf16[32,2048]{1,0:T(8,128)(2,1)}, u32[]{:S(2)}) copy-start(bf16[32,2048]{1,0:T(8,128)(2,1)} %param.14) | copy-start | bytes 393220
  167.7 1.9 copy-start
  171.6 11.9 %all-to-all-start.5 = ((f32[8,128,2]{1,2,0:T(2,128)}), f32[8,128,2]{1,2,0:T(2,128)S(1)}, u32[]{:S(2)}, u32[]{:S(2)}) async-start(f32[8,128,2]{1,2,0:T(2,128)} %bitcast.40), calls=%async_computation.6 | async-start | bytes 16384 | tf_op jit(solution)/shard_map/all_to_all | solution.py:120
  183.5 9.9 %all-to-all-start.3 = ((f32[8,128,2]{1,2,0:T(2,128)}), f32[8,128,2]{1,2,0:T(2,128)S(1)}, u32[]{:S(2)}, u32[]{:S(2)}) async-start(f32[8,128,2]{1,2,0:T(2,128)} %bitcast.31), calls=%async_computation.4 | async-start | bytes 16384 | tf_op jit(solution)/shard_map/all_to_all | solution.py:119
  187.0 20.6 %copy-start.3 = (bf16[2,256,2048]{2,1,0:T(8,128)(2,1)S(1)}, bf16[2,256,2048]{2,1,0:T(8,128)(2,1)}, u32[]{:S(2)}) copy-start(bf16[2,256,2048]{2,1,0:T(8,128)(2,1)} %param.21) | copy-start | bytes 6291460
  190.3 18.7 %copy-start.5 = (bf16[2048]{0:T(1024)(128)(2,1)S(1)}, bf16[2048]{0:T(1024)(128)(2,1)}, u32[]{:S(2)}) copy-start(bf16[2048]{0:T(1024)(128)(2,1)} %param.22) | copy-start | bytes 12292
  193.4 14.0 %all-to-all-start.4 = ((bf16[8,128,2,128]{1,3,2,0:T(8,128)(2,1)}), bf16[8,128,2,128]{1,3,2,0:T(8,128)(2,1)S(1)}, u32[]{:S(2)}, u32[]{:S(2)}) async-start(bf16[8,128,2,128]{1,3,2,0:T(8,128)(2,1)} %copy.32), calls=%async_computation.5 | async-start | bytes 1048576 | tf_op jit(solution)/shard_map/all_to_all | solution.py:116
  197.1 35.6 %reduce-scatter.6.cloned.1.call-start = ((), (), s32[]{:S(2)}) async-start(), calls=%async_computation.11 | async-start | bytes 1310720 | tf_op jit(solution)/shard_map/reduce_scatter | solution.py:135
  209.0 67.9 %reduce-scatter.8.cloned.1.call-start = ((), (), s32[]{:S(2)}) async-start(), calls=%async_computation.12 | async-start | bytes 1310720 | tf_op jit(solution)/shard_map/reduce_scatter | solution.py:150
Sparse Core Ops, SparseCore 0:
  8.9 25.2 all-gather.1
  102.0 23.3 reduce-scatter.3
  209.1 23.5 reduce-scatter.5
  251.5 25.2 reduce-scatter.7
where the time goes:
time: 286 us; the launch traced here: 285 us
  waiting for transfers between devices  105 us (37%)
  blocking collectives  85 us (30%)
  matrix products  36.4 us (13%)
  starting transfers between devices  25.1 us (9%)
  other arithmetic  14.4 us (5%)
  between operations  13.4 us (5%)
  local copies, waits for them, and re-layouts  5.88 us (2%)
    all_gather x2, blocking collectives, local(): everyone = lax.all_gather(queries, 'sp', axis=0, tiled=True)  63.2 us
    reduce_scatter x2, waiting for transfers between devices, local(): lax.psum_scatter(mix_heads(jnp.int32(0), own_rows * lax.axis_size('tp')),...  45 us
    reduce_scatter x1, waiting for transfers between devices, local(): lax.psum_scatter(jnp.dot(hidden, down_weight, preferred_element_type=jnp....  25.4 us
    all_to_all x2, waiting for transfers between devices, local(): lax.all_to_all(outgoing[0].astype(jnp.float32), 'sp', split_axis=0, conca...  20.3 us
    all_gather x2, blocking collectives, local(): lax.all_gather(tgt_normed, 'tp', axis=0, tiled=True)  15.3 us
    all_to_all x2, starting transfers between devices, local(): lax.all_to_all(outgoing[2], 'sp', split_axis=0, concat_axis=0, tiled=True)  11 us
    all_to_all x2, waiting for transfers between devices, local(): lax.all_to_all(outgoing[2], 'sp', split_axis=0, concat_axis=0, tiled=True)  8.72 us
    dot_general x1, matrix products, local(): jnp.dot(hidden, down_weight, preferred_element_type=jnp.float32)  7.25 us
  transfers between devices with their start and end apart: 10, of which 9 were waited for; matrix products, arithmetic and copies ran while one was open for 7% of the time, Pallas kernels for 0%

commit v1 on v0

v1 whole, which is shorter than its diff:
```python
import functools

import jax
import jax.numpy as jnp
from jax import lax
from jax.experimental import pallas as pl
from jax.experimental.pallas import tpu as pltpu
from jax.sharding import PartitionSpec as P

HEAD_DIM = 128
EPSILON = 1e-06
LOG2E = 1.4426950408889634
CHUNKS = 4
TILE = 256
BF = jnp.bfloat16
F32 = jnp.float32


def rms(rows):
    return rows * lax.rsqrt(jnp.mean(rows * rows, axis=-1, keepdims=True) + EPSILON)


def dot(a, b):
    return jnp.dot(a, b, preferred_element_type=F32)


def dot_nt(a, b):
    return lax.dot_general(a, b, (((1,), (1,)), ((), ())), preferred_element_type=F32)


def merge(parts):
    top = functools.reduce(jnp.maximum, [m for _, m, _ in parts])
    out, total = 0.0, 0.0
    for o, m, t in parts:
        factor = jnp.exp2(m - top)
        out = out + factor * o.astype(F32)
        total = total + factor * t
    return out, top, total


def kernel(
    n_sp, n_tp,
    target, source_gain, target_gain, head_gain, mlp_gain,
    source, *rest,
):
    weights_hbm = rest[:7]
    out_ref = rest[7]
    (src, xs, qw, kw, vw, ow, gw, uw, dw, nrm, kbuf, vbuf, qbuf, head,
     o_own, s_own, o_snd, s_snd, o_p1, s_p1, o_mrg, s_mrg, o_r2, s_r2,
     r_own, r_snd, r_p1, r_mrg, r_r2, hid, load_sem, send_sem, recv_sem) = rest[8:]
    layers = qw.shape[0]
    heads = qw.shape[2] // HEAD_DIM
    width = xs.shape[3]
    rows = xs.shape[2]
    group = rows * n_tp
    src_rows = src.shape[1]
    cols = width // CHUNKS
    n_x, n_p = n_tp // 2, n_sp // 2
    sp, tp = lax.axis_index("sp"), lax.axis_index("tp")
    where = {"sp": (sp // 2, sp % 2, n_p), "tp": (tp // 2, tp % 2, n_x)}

    def peer(axis, shift):
        pair, side, count = where[axis]
        return {axis: ((pair + shift + count) % count) * 2 + side}

    def partner(axis):
        pair, side, _ = where[axis]
        return {axis: pair * 2 + 1 - side}

    copies = []

    def remote(src_ref, dst_ref, device):
        number = len(copies)
        copy = pltpu.make_async_remote_copy(
            src_ref=src_ref, dst_ref=dst_ref,
            send_sem=send_sem.at[number], recv_sem=recv_sem.at[number],
            device_id=device, device_id_type=pl.DeviceIdType.MESH,
        )
        copy.start()
        copies.append(copy)
        return copy

    loads = {}

    def load(name, src_ref, dst_ref):
        copy = pltpu.make_async_copy(src_ref, dst_ref, load_sem.at[len(loads)])
        copy.start()
        loads[name] = copy

    qh, kh, vh, oh, gh, uh, dh = weights_hbm
    load("src", source, src.at[0])
    for l in range(layers):
        load(("q", l), qh.at[l], qw.at[l])
        load(("k", l), kh.at[l], kw.at[l])
        load(("v", l), vh.at[l], vw.at[l])
        load(("o", l), oh.at[l], ow.at[l])
    load("g", gh, gw)
    load("u", uh, uw)
    load("d", dh, dw)

    barrier = pltpu.get_barrier_semaphore()
    others = [peer("tp", k) for k in range(1, n_x)] + [peer("sp", k) for k in range(1, n_p)]
    others += [partner("tp"), partner("sp")]
    for device in others:
        pl.semaphore_signal(barrier, inc=1, device_id=device, device_id_type=pl.DeviceIdType.MESH)
    pl.semaphore_wait(barrier, len(others))

    class Gather:
        def __init__(self, own, buf, axis):
            self.buf, self.axis = buf, axis
            self.count = where[axis][2]
            self.far = {k: remote(own, buf.at[2 * k], peer(axis, k)) for k in range(1, self.count)}
            self.near = {0: remote(own, buf.at[1], partner(axis))}

        def forward(self, k):
            self.far[k].wait_recv()
            self.near[k] = remote(
                self.buf.at[2 * k], self.buf.at[2 * k + 1], partner(self.axis)
            )

        def forward_all(self):
            for k in range(1, self.count):
                self.forward(k)

        def wait_near(self, k):
            self.near[k].wait_recv()

        def wait_all(self):
            for k in range(self.count):
                self.wait_near(k)

    def project_source(layer, slot):
        normed = rms(src[slot].astype(F32)) * source_gain[pl.ds(layer, 1), :].astype(F32)
        normed = normed.astype(BF)
        span = pl.ds(slot * src_rows, src_rows)
        kbuf[span, :] = dot(normed, kw[layer]).astype(BF)
        vbuf[:, span] = dot(normed, vw[layer]).T.astype(BF)

    def attend(layer, slot):
        parts = []
        for h in range(heads):
            span = pl.ds(h * HEAD_DIM, HEAD_DIM)
            scores = dot_nt(kbuf[:, span], qbuf[layer, slot, :, span]) * (
                HEAD_DIM ** (-0.5) * LOG2E
            )
            top = jnp.max(scores, axis=0, keepdims=True)
            weights = jnp.exp2(scores - top)
            total = jnp.sum(weights, axis=0, keepdims=True)
            parts.append((dot(vbuf[span, :], weights.astype(BF)), top, total))
        return parts

    def put(parts, out, stats):
        for h, (o, m, t) in enumerate(parts):
            out[pl.ds(h * HEAD_DIM, HEAD_DIM), :] = o.astype(out.dtype)
            stats[pl.ds(h, 1), :] = m
            stats[pl.ds(heads + h, 1), :] = t

    def get(out, stats, h):
        return (
            out[pl.ds(h * HEAD_DIM, HEAD_DIM), :],
            stats[pl.ds(h, 1), :],
            stats[pl.ds(heads + h, 1), :],
        )

    def reduce_scatter(phase, part):
        first, second = {}, {}

        def pass_on(j):
            for k in range(1, n_x):
                first[j, k].wait_recv()
                r_mrg[phase, j, k] = (
                    r_own[k, :, pl.ds(j * cols, cols)] + r_p1[phase, j, k].astype(F32)
                ).astype(BF)
                second[j, k] = remote(
                    r_mrg.at[phase, j, k], r_r2.at[phase, j, k], peer("tp", -k)
                )

        for j in range(CHUNKS):
            piece = part(j)
            for k in list(range(1, n_x)) + [0]:
                mine, other = 2 * k * rows, (2 * k + 1) * rows
                r_own[k, :, pl.ds(j * cols, cols)] = piece[mine : mine + rows]
                r_snd[phase, j, k] = piece[other : other + rows].astype(BF)
                first[j, k] = remote(r_snd.at[phase, j, k], r_p1.at[phase, j, k], partner("tp"))
            if j:
                pass_on(j - 1)
        pass_on(CHUNKS - 1)
        for j in range(CHUNKS):
            first[j, 0].wait_recv()
            total = r_own[0, :, pl.ds(j * cols, cols)] + r_p1[phase, j, 0].astype(F32)
            for k in range(1, n_x):
                second[j, k].wait_recv()
                total = total + r_r2[phase, j, k].astype(F32)
            yield pl.ds(j * cols, cols), total

    def norm_rows(phase, gain):
        for s in range(n_tp):
            nrm[pl.ds(s * rows, rows), :] = (rms(xs[phase, s].astype(F32)) * gain).astype(BF)

    rows_in = Gather(target, xs.at[0], "tp")
    xs[0, 0] = target[...]
    loads["src"].wait()
    source_in = Gather(src.at[0], src, "tp")

    for l in range(layers):
        rows_in.forward_all()
        rows_in.wait_all()
        norm_rows(l, target_gain[pl.ds(l, 1), :].astype(F32))
        loads["q", l].wait()
        qbuf[l, 0] = dot(nrm[...], qw[l]).astype(BF)
        queries = Gather(qbuf.at[l, 0], qbuf.at[l], "sp")
        if l == 0:
            loads["k", l].wait()
            loads["v", l].wait()
            project_source(l, 0)
            source_in.wait_near(0)
            project_source(l, 1)
        queries.forward_all()
        if l == 0:
            source_in.forward_all()
            for k in range(1, n_x):
                project_source(l, 2 * k)
                source_in.wait_near(k)
                project_source(l, 2 * k + 1)
        near_o, near_s, far_o, far_s = {}, {}, {}, {}

        def pass_on(k, l=l, near_o=near_o, near_s=near_s, far_o=far_o, far_s=far_s):
            near_o[k].wait_recv()
            near_s[k].wait_recv()
            merged = [
                merge([get(o_own.at[k], s_own.at[k], h), get(o_p1.at[l, k], s_p1.at[l, k], h)])
                for h in range(heads)
            ]
            put(merged, o_mrg.at[l, k], s_mrg.at[l, k])
            far_s[k] = remote(s_mrg.at[l, k], s_r2.at[l, k], peer("sp", -k))
            far_o[k] = remote(o_mrg.at[l, k], o_r2.at[l, k], peer("sp", -k))

        order = list(range(1, n_p)) + [0]
        for step, k in enumerate(order):
            put(attend(l, 2 * k), o_own.at[k], s_own.at[k])
            queries.wait_near(k)
            put(attend(l, 2 * k + 1), o_snd.at[l, k], s_snd.at[l, k])
            near_s[k] = remote(s_snd.at[l, k], s_p1.at[l, k], partner("sp"))
            near_o[k] = remote(o_snd.at[l, k], o_p1.at[l, k], partner("sp"))
            if step:
                pass_on(order[step - 1])
        if l + 1 < layers:
            loads["k", l + 1].wait()
            loads["v", l + 1].wait()
            for slot in range(n_tp):
                project_source(l + 1, slot)
        near_o[0].wait_recv()
        near_s[0].wait_recv()
        for k in range(1, n_p):
            far_s[k].wait_recv()
            far_o[k].wait_recv()
        for h in range(heads):
            parts = [get(o_own.at[0], s_own.at[0], h), get(o_p1.at[l, 0], s_p1.at[l, 0], h)]
            parts += [get(o_r2.at[l, k], s_r2.at[l, k], h) for k in range(1, n_p)]
            out, _, total = merge(parts)
            attended = out / total
            attended = attended * lax.rsqrt(
                jnp.mean(attended * attended, axis=0, keepdims=True) + EPSILON
            )
            span = pl.ds(h * HEAD_DIM, HEAD_DIM)
            head[:, span] = (
                attended.T * head_gain[pl.ds(l, 1), span].astype(F32)
            ).astype(BF)
        loads["o", l].wait()

        def share(j, l=l):
            return dot(head[...], ow[l, :, pl.ds(j * cols, cols)])

        for span, total in reduce_scatter(l, share):
            xs[l + 1, 0, :, span] = (xs[l, 0, :, span].astype(F32) + total).astype(BF)
        rows_in = Gather(xs.at[l + 1, 0], xs.at[l + 1], "tp")

    rows_in.forward_all()
    rows_in.wait_all()
    norm_rows(layers, mlp_gain[...].astype(F32))
    loads["g"].wait()
    loads["u"].wait()
    units = gw.shape[1]
    for begin in range(0, units, TILE):
        span = pl.ds(begin, min(TILE, units - begin))
        gate = dot(nrm[...], gw[:, span])
        upward = dot(nrm[...], uw[:, span])
        hid[:, span] = (gate / (1.0 + jnp.exp(-gate)) * upward).astype(BF)
    loads["d"].wait()

    def down(j):
        return dot(hid[...], dw[:, pl.ds(j * cols, cols)])

    for span, total in reduce_scatter(layers, down):
        out_ref[:, span] = (xs[layers, 0, :, span].astype(F32) + 0.5 * total).astype(BF)
    for copy in copies:
        copy.wait_send()


def local(
    n_sp, n_tp,
    source, target, source_gain, target_gain, query_weight, key_weight, value_weight,
    head_gain, out_weight, mlp_gain, gate_weight, up_weight, down_weight,
):
    layers, width, qwidth = query_weight.shape
    rows, src_rows, units = target.shape[0], source.shape[0], gate_weight.shape[1]
    group, n_x, n_p = rows * n_tp, n_tp // 2, n_sp // 2
    cols = width // CHUNKS
    total = (layers + 2) * (2 * n_x - 1) + layers * 3 * (2 * n_p - 1)
    total += (layers + 1) * CHUNKS * (2 * n_x - 1)
    vm = pltpu.VMEM
    wide, thin = (layers, n_p, qwidth, group), (layers, n_p, 8, group)
    summed = (layers + 1, CHUNKS, n_x, rows, cols)
    scratch = [
        vm((n_tp, src_rows, width), BF),
        vm((layers + 1, n_tp, rows, width), BF),
        vm((layers, width, qwidth), BF),
        vm((layers, width, qwidth), BF),
        vm((layers, width, qwidth), BF),
        vm((layers, qwidth, width), BF),
        vm((width, units), BF),
        vm((width, units), BF),
        vm((units, width), BF),
        vm((group, width), BF),
        vm((n_tp * src_rows, qwidth), BF),
        vm((qwidth, n_tp * src_rows), BF),
        vm((layers, n_sp, group, qwidth), BF),
        vm((group, qwidth), BF),
        vm(wide[1:], F32), vm(thin[1:], F32),
        vm(wide, BF), vm(thin, F32),
        vm(wide, BF), vm(thin, F32),
        vm(wide, BF), vm(thin, F32),
        vm(wide, BF), vm(thin, F32),
        vm((n_x, rows, width), F32),
        vm(summed, BF), vm(summed, BF), vm(summed, BF), vm(summed, BF),
        vm((group, units), BF),
        pltpu.SemaphoreType.DMA((4 * layers + 4,)),
        pltpu.SemaphoreType.DMA((total,)),
        pltpu.SemaphoreType.DMA((total,)),
    ]
    inside = pl.BlockSpec(memory_space=pltpu.VMEM)
    outside = pl.BlockSpec(memory_space=pl.ANY)
    return pl.pallas_call(
        functools.partial(kernel, n_sp, n_tp),
        out_shape=jax.ShapeDtypeStruct((rows, width), BF),
        in_specs=[inside] * 5 + [outside] * 8,
        out_specs=inside,
        scratch_shapes=scratch,
        compiler_params=pltpu.CompilerParams(
            collective_id=0, has_side_effects=True, vmem_limit_bytes=60 * 1024 * 1024
        ),
        name="decoder_step",
    )(
        target, source_gain, target_gain, head_gain, mlp_gain.reshape(1, width),
        source, query_weight, key_weight, value_weight, out_weight,
        gate_weight, up_weight, down_weight,
    )


def solution(mesh):
    in_specs = (
        P(("sp", "tp"), None),
        P(("sp", "tp"), None),
        P(),
        P(),
        P(None, None, "tp"),
        P(None, None, "tp"),
        P(None, None, "tp"),
        P(None, "tp"),
        P(None, "tp", None),
        P(),
        P(None, "tp"),
        P(None, "tp"),
        P("tp", None),
    )
    out_specs = P(("sp", "tp"), None)
    run = functools.partial(local, mesh.shape["sp"], mesh.shape["tp"])
    return jax.shard_map(run, mesh=mesh, in_specs=in_specs, out_specs=out_specs, check_vma=False)
```

time: 286 us -> 96 us (0.34)
  waiting for transfers between devices: 105 us -> 0 us
  Pallas kernels: 0 us -> 92.7 us
  blocking collectives: 85 us -> 0 us
  matrix products: 36.4 us -> 0 us
  starting transfers between devices: 25.1 us -> 0 us
  other arithmetic: 14.4 us -> 0 us
  between operations: 13.4 us -> 0.01 us
  local copies, waits for them, and re-layouts: 5.88 us -> 2.86 us
    pallas_call x0 -> x1, Pallas kernels: none -> 92.7 us  [local(): pl.pallas_call(functools.partial(kernel, n_sp, n_tp), out_shape=jax.Shape...]
    all_gather x5 -> x0, blocking collectives: 85 us -> none  [the longest x2 63.2 us: local(): everyone = lax.all_gather(queries, 'sp', axis=0, tiled=True)]
    reduce_scatter x3 -> x0, waiting for transfers between devices: 70.4 us -> none  [the longest x2 45 us: local(): lax.psum_scatter(mix_heads(jnp.int32(0), own_rows * lax.axis_size('tp')),...]
    dot_general x14 -> x0, matrix products: 36.4 us -> none  [the longest x1 7.25 us: local(): jnp.dot(hidden, down_weight, preferred_element_type=jnp.float32)]
    all_to_all x6 -> x0, waiting for transfers between devices: 33.6 us -> none  [the longest x2 20.3 us: local(): lax.all_to_all(outgoing[0].astype(jnp.float32), 'sp', split_axis=0, conca...]
    all_to_all x6 -> x0, starting transfers between devices: 25 us -> none  [the longest x2 11 us: local(): lax.all_to_all(outgoing[2], 'sp', split_axis=0, concat_axis=0, tiled=True)]
    reduce_sum x12 -> x0, other arithmetic: 9.67 us -> none  [the longest x6 5.39 us: row_scale(): return lax.rsqrt(jnp.mean(rows * rows, axis=-1, keepdims=True) + EPSILON)]
    convert_element_type x8 -> x0, other arithmetic: 3.06 us -> none  [the longest x1 1.64 us: local(): return (state_wide + 0.5 * down).astype(jnp.bfloat16)]
  transfers between devices with their start and end apart: 10 -> 0, of which waited for: 9 -> 0; matrix products, arithmetic and copies ran while one was open for 7% -> 0% of each run, Pallas kernels for 0% -> 0%
where the time goes in v1:
time: 96 us; the launch traced here: 95.6 us
  Pallas kernels  92.7 us (97%)
  local copies, waits for them, and re-layouts  2.86 us (3%)
    pallas_call x1, Pallas kernels, local(): pl.pallas_call(functools.partial(kernel, n_sp, n_tp), out_shape=jax.Shape...  92.7 us

profile of v1, /device:TPU:0, one launch (start us, length us, event | category | flops | bytes accessed | tf_op | source)
XLA Modules:
  0.0 95.6 jit_solution(15159244822125643004)
XLA Ops:
  0.0 1.3 %reshape.3.mlp_gain = bf16[1,2048]{1,0:T(2,128)(2,1)} reshape(bf16[2048]{0:T(1024)(128)(2,1)} %param.22) | data formatting | bytes 8192 | tf_op jit(solution)/shard_map/reshape | solution.py:354
  1.3 92.7 %decoder_step.1 = bf16[32,2048]{1,0:T(8,128)(2,1)} custom-call(bf16[32,2048]{1,0:T(8,128)(2,1)} %target.1, bf16[2,2048]{1,0:T(2,128)(2,1)} %source_gain.1, bf16[2,2048]{1,0:T(2,128)(2,1)} %target_gain.1, bf16[2,256]{1,0:T(2,128)(2,1)} %head_gain.1, bf16[1,2048]{1,0:T(2,128)(2,1)} %reshape.3.mlp_gain, bf16[128,2048]{1,0:T(8,128)(2,1)} %source.1, ...), custom_call_target="tpu_custom_call" | custom-call | tf_op jit(solution)/shard_map/decoder_step/pallas_call | solution.py:343
  94.0 1.6 %copy.15 = bf16[32,2048]{1,0:T(8,128)(2,1)} copy(bf16[32,2048]{1,0:T(8,128)(2,1)} %decoder_step.1) | data formatting | bytes 262144

commit v2 on v1

--- a/solution.py
+++ b/solution.py
@@ -129,6 +129,37 @@
             for k in range(self.count):
                 self.wait_near(k)
 
+    class RowGather:
+        def __init__(self, phase):
+            self.phase = phase
+            self.far, self.near = {}, {}
+
+        def part(self, slot, j):
+            return xs.at[self.phase, slot, :, pl.ds(j * cols, cols)]
+
+        def send(self, j):
+            for k in range(1, n_x):
+                self.far[j, k] = remote(self.part(0, j), self.part(2 * k, j), peer("tp", k))
+            self.near[j, 0] = remote(self.part(0, j), self.part(1, j), partner("tp"))
+
+        def normalize(self, gain):
+            def norm(slot):
+                piece = rms(xs[self.phase, slot].astype(F32)) * gain
+                nrm[pl.ds(slot * rows, rows), :] = piece.astype(BF)
+
+            norm(0)
+            for k in range(n_x):
+                if k:
+                    for j in range(CHUNKS):
+                        self.far[j, k].wait_recv()
+                        self.near[j, k] = remote(
+                            self.part(2 * k, j), self.part(2 * k + 1, j), partner("tp")
+                        )
+                    norm(2 * k)
+                for j in range(CHUNKS):
+                    self.near[j, k].wait_recv()
+                norm(2 * k + 1)
+
     def project_source(layer, slot):
         normed = rms(src[slot].astype(F32)) * source_gain[pl.ds(layer, 1), :].astype(F32)
         normed = normed.astype(BF)
@@ -193,19 +224,15 @@
                 total = total + r_r2[phase, j, k].astype(F32)
             yield pl.ds(j * cols, cols), total
 
-    def norm_rows(phase, gain):
-        for s in range(n_tp):
-            nrm[pl.ds(s * rows, rows), :] = (rms(xs[phase, s].astype(F32)) * gain).astype(BF)
-
-    rows_in = Gather(target, xs.at[0], "tp")
     xs[0, 0] = target[...]
+    rows_in = RowGather(0)
+    for j in range(CHUNKS):
+        rows_in.send(j)
     loads["src"].wait()
     source_in = Gather(src.at[0], src, "tp")
 
     for l in range(layers):
-        rows_in.forward_all()
-        rows_in.wait_all()
-        norm_rows(l, target_gain[pl.ds(l, 1), :].astype(F32))
+        rows_in.normalize(target_gain[pl.ds(l, 1), :].astype(F32))
         loads["q", l].wait()
         qbuf[l, 0] = dot(nrm[...], qw[l]).astype(BF)
         queries = Gather(qbuf.at[l, 0], qbuf.at[l], "sp")
@@ -215,8 +242,8 @@
             project_source(l, 0)
             source_in.wait_near(0)
             project_source(l, 1)
-        queries.forward_all()
         if l == 0:
+            queries.forward_all()
             source_in.forward_all()
             for k in range(1, n_x):
                 project_source(l, 2 * k)
@@ -235,15 +262,31 @@
             far_s[k] = remote(s_mrg.at[l, k], s_r2.at[l, k], peer("sp", -k))
             far_o[k] = remote(o_mrg.at[l, k], o_r2.at[l, k], peer("sp", -k))
 
-        order = list(range(1, n_p)) + [0]
-        for step, k in enumerate(order):
-            put(attend(l, 2 * k), o_own.at[k], s_own.at[k])
+        def attend_near(k, l=l, queries=queries):
             queries.wait_near(k)
             put(attend(l, 2 * k + 1), o_snd.at[l, k], s_snd.at[l, k])
+
+        def send_near(k, l=l, near_o=near_o, near_s=near_s):
             near_s[k] = remote(s_snd.at[l, k], s_p1.at[l, k], partner("sp"))
             near_o[k] = remote(o_snd.at[l, k], o_p1.at[l, k], partner("sp"))
-            if step:
-                pass_on(order[step - 1])
+
+        def forward(k, l=l, queries=queries):
+            if l and k < n_p:
+                queries.forward(k)
+
+        put(attend(l, 0), o_own.at[0], s_own.at[0])
+        forward(1)
+        attend_near(0)
+        forward(2)
+        for k in range(1, n_p):
+            put(attend(l, 2 * k), o_own.at[k], s_own.at[k])
+            forward(k + 2)
+            attend_near(k)
+            send_near(k)
+            if k > 1:
+                pass_on(k - 1)
+        send_near(0)
+        pass_on(n_p - 1)
         if l + 1 < layers:
             loads["k", l + 1].wait()
             loads["v", l + 1].wait()
@@ -271,13 +314,12 @@
         def share(j, l=l):
             return dot(head[...], ow[l, :, pl.ds(j * cols, cols)])
 
-        for span, total in reduce_scatter(l, share):
+        rows_in = RowGather(l + 1)
+        for j, (span, total) in enumerate(reduce_scatter(l, share)):
             xs[l + 1, 0, :, span] = (xs[l, 0, :, span].astype(F32) + total).astype(BF)
-        rows_in = Gather(xs.at[l + 1, 0], xs.at[l + 1], "tp")
-
-    rows_in.forward_all()
-    rows_in.wait_all()
-    norm_rows(layers, mlp_gain[...].astype(F32))
+            rows_in.send(j)
+
+    rows_in.normalize(mlp_gain[...].astype(F32).reshape(1, width))
     loads["g"].wait()
     loads["u"].wait()
     units = gw.shape[1]
@@ -306,7 +348,7 @@
     rows, src_rows, units = target.shape[0], source.shape[0], gate_weight.shape[1]
     group, n_x, n_p = rows * n_tp, n_tp // 2, n_sp // 2
     cols = width // CHUNKS
-    total = (layers + 2) * (2 * n_x - 1) + layers * 3 * (2 * n_p - 1)
+    total = ((layers + 1) * CHUNKS + 1) * (2 * n_x - 1) + layers * 3 * (2 * n_p - 1)
     total += (layers + 1) * CHUNKS * (2 * n_x - 1)
     vm = pltpu.VMEM
     wide, thin = (layers, n_p, qwidth, group), (layers, n_p, 8, group)
@@ -351,7 +393,7 @@
         ),
         name="decoder_step",
     )(
-        target, source_gain, target_gain, head_gain, mlp_gain.reshape(1, width),
+        target, source_gain, target_gain, head_gain, mlp_gain,
         source, query_weight, key_weight, value_weight, out_weight,
         gate_weight, up_weight, down_weight,
     )

time: 96 us -> 94.2 us (0.981)
  local copies, waits for them, and re-layouts: 2.86 us -> 1.57 us
    reshape x1 -> x0, local copies, waits for them, and re-layouts: 1.29 us -> none  [local(): mlp_gain.reshape(1, width)]
where the time goes in v2:
time: 94.2 us; the launch traced here: 94.1 us
  Pallas kernels  92.5 us (98%)
  local copies, waits for them, and re-layouts  1.57 us (2%)
    pallas_call x1, Pallas kernels, local(): pl.pallas_call(functools.partial(kernel, n_sp, n_tp), out_shape=jax.Shape...  92.5 us

profile of v2, /device:TPU:0, one launch (start us, length us, event | category | flops | bytes accessed | tf_op | source)
XLA Modules:
  0.0 94.1 jit_solution(884227525351361049)
XLA Ops:
  0.0 92.5 %decoder_step.1 = bf16[32,2048]{1,0:T(8,128)(2,1)} custom-call(bf16[32,2048]{1,0:T(8,128)(2,1)} %target.1, bf16[2,2048]{1,0:T(2,128)(2,1)} %source_gain.1, bf16[2,2048]{1,0:T(2,128)(2,1)} %target_gain.1, bf16[2,256]{1,0:T(2,128)(2,1)} %head_gain.1, bf16[2048]{0:T(1024)(128)(2,1)} %mlp_gain.1, bf16[128,2048]{1,0:T(8,128)(2,1)} %source.1, ...), custom_call_target="tpu_custom_call" | custom-call | tf_op jit(solution)/shard_map/decoder_step/pallas_call | solution.py:385
  92.5 1.6 %copy.15 = bf16[32,2048]{1,0:T(8,128)(2,1)} copy(bf16[32,2048]{1,0:T(8,128)(2,1)} %decoder_step.1) | data formatting | bytes 262144
